TPU v7x, 512 devices: a whole 4x8x8 slice. The times are simulated.
512 devices in a mesh: ep: 128 (over z, y, core), tp: 4 (over x).
Axes of the slice: x: 4, y: 8, z: 8, core: 2. Of those that a mesh axis runs over, the one named last changes fastest.
Arguments:
- tokens: bfloat16 [2048, 1024], P('ep', 'tp'), may hold values from -75 to 75
- gain_mix: float32 [1024], replicated, may hold values from 0.1 to 1.9
- w_query: bfloat16 [1024, 512], P(None, 'tp'), may hold values from -0.1875 to 0.1875
- w_key: bfloat16 [1024, 512], P(None, 'tp'), may hold values from -0.1875 to 0.1875
- w_value: bfloat16 [1024, 512], P(None, 'tp'), may hold values from -0.1875 to 0.1875
- w_outgate: bfloat16 [1024, 512], P(None, 'tp'), may hold values from -0.1875 to 0.1875
- w_input_gate: bfloat16 [1024, 4], P(None, 'tp'), may hold values from -0.1875 to 0.1875
- w_forget_gate: bfloat16 [1024, 4], P(None, 'tp'), may hold values from -0.1875 to 0.1875
- w_mix_out: bfloat16 [512, 1024], P(None, 'tp'), may hold values from -0.25 to 0.25
- cell_state: float32 [2048, 4, 128, 128], P('ep', 'tp'), may hold values from -3 to 3
- norm_state: float32 [2048, 4, 128], P('ep', 'tp'), may hold values from -3 to 3
- max_state: float32 [2048, 4], P('ep', 'tp'), may hold values from -2 to 143
- gain_ffn: float32 [1024], replicated, may hold values from 0.1 to 1.9
- route_ids: int32 [2048, 2], P('ep'), may hold values from 0 to 127, all different within a row; in each aligned block of 16 rows (0 to 15, 16 to 31, ...) no two rows name the same one
- route_logits: float32 [2048, 2], P('ep'), may hold values from -5 to 5
- expert_gate: bfloat16 [128, 1024, 1408], P('ep', None, 'tp'), may hold values from -0.1875 to 0.1875
- expert_up: bfloat16 [128, 1024, 1408], P('ep', None, 'tp'), may hold values from -0.1875 to 0.1875
- expert_down: bfloat16 [128, 1408, 1024], P('ep', 'tp'), may hold values from -0.15625 to 0.15625
- dense_gate: bfloat16 [1024, 3072], P('tp', 'ep'), may hold values from -0.1875 to 0.1875
- dense_up: bfloat16 [1024, 3072], P('tp', 'ep'), may hold values from -0.1875 to 0.1875
- dense_down: bfloat16 [3072, 1024], P('ep', 'tp'), may hold values from -0.3125 to 0.3125
- dense_mix: bfloat16 [1024], P('tp'), may hold values from -0.1875 to 0.1875
Outputs:
- layer_out: bfloat16 [2048, 1024], P('ep', 'tp')
Inputs may be any that keep to these rules, and one draw needn't show every extreme that they name: `route_ids`: each row names 2 different experts. Among the 16 tokens of one index of ep no expert is named more than 1 times, and in every draw some expert is named exactly 1 times by the tokens of one index of ep.
All inputs are finite; a program needn't handle non-finite values.
Results may differ from a plain program's by a relative error of at most 0.013.
Values may be sent and summed in bfloat16 or wider, within the bound.
No kernel may reach another device: no remote copies, remote signals or barrier semaphores. Data moves between devices by JAX's collectives and lax.ppermute only.
A program may use at most 64 MiB of HBM per device.

v0:
```python
import jax
import jax.numpy as jnp
from jax import lax
from jax.sharding import PartitionSpec as P

HEAD = 128
TOP = 2
epsilon = 1e-06
highest = lax.Precision.HIGHEST


def sent_to_all(shard, axis):
    size = lax.axis_size(axis)
    return lax.all_to_all(
        jnp.broadcast_to(shard[None], (size, *shard.shape)), axis, 0, 0, tiled=True
    )


def joined_along(blocks, dim):
    dims = list(blocks.shape[1:])
    dims[dim] *= blocks.shape[0]
    return jnp.moveaxis(blocks, 0, dim).reshape(dims)


def collect(shard, axis, dim):
    blocks = sent_to_all(shard, axis)
    return joined_along(blocks, dim)


def cut_along(shard, dim, size):
    dims = shard.shape
    blocks = shard.reshape(*dims[:dim], size, dims[dim] // size, *dims[dim + 1 :])
    return jnp.moveaxis(blocks, dim, 0)


def sent_and_summed(shard, axis, dim):
    blocks = cut_along(shard, dim, lax.axis_size(axis))
    arrived = lax.all_to_all(blocks, axis, split_axis=0, concat_axis=0, tiled=True)
    return arrived.astype(jnp.float32).sum(axis=0)


def turned_gather(arrays, axis, dims):
    turned = [jnp.moveaxis(a, dim, 0) for a, dim in zip(arrays, dims)]
    widths = [t[0].size for t in turned]
    both = jnp.concatenate([t.reshape(-1, w) for t, w in zip(turned, widths)], axis=1)
    result = lax.all_gather(both, axis, axis=0, tiled=True)
    blocks = jnp.split(result, [sum(widths[:k]) for k in range(1, len(widths))], axis=1)
    return tuple(
        (
            jnp.moveaxis(b.reshape(-1, *t.shape[1:]), 0, dim)
            for b, t, dim in zip(blocks, turned, dims)
        )
    )


def of_everyone(shard, axis):
    return sent_to_all(shard, axis).astype(jnp.float32).sum(axis=0)


def rms_norm(rows, gain):
    values = rows.astype(jnp.float32)
    scale = lax.rsqrt(jnp.mean(values * values, axis=-1, keepdims=True) + epsilon)
    return (values * scale * gain).astype(jnp.bfloat16)


def local(
    tokens,
    gain_mix,
    w_query,
    w_key,
    w_value,
    w_outgate,
    w_input_gate,
    w_forget_gate,
    w_mix_out,
    cell_state,
    norm_state,
    max_state,
    gain_ffn,
    route_ids,
    route_logits,
    expert_gate,
    expert_up,
    expert_down,
    dense_gate,
    dense_up,
    dense_down,
    dense_mix,
):
    seq_count, quarter = tokens.shape
    tp_rank = lax.axis_index("tp")
    full_tokens = collect(tokens, "tp", 1)
    normed_mix = rms_norm(full_tokens, gain_mix)

    def project(weight):
        return jnp.dot(normed_mix, weight, preferred_element_type=jnp.float32)

    query_rows = project(w_query).reshape(seq_count, -1, HEAD)
    key_rows = project(w_key).reshape(seq_count, -1, HEAD) * HEAD ** (-0.5)
    value_rows = project(w_value).reshape(seq_count, -1, HEAD)
    out_gate = project(w_outgate)
    input_gate = project(w_input_gate)
    carried = jax.nn.log_sigmoid(project(w_forget_gate)) + max_state
    stabilizer = jnp.maximum(carried, input_gate)
    weight_old = jnp.exp(carried - stabilizer)
    weight_new = jnp.exp(input_gate - stabilizer) * jnp.sum(query_rows * key_rows, axis=-1)
    cell_read = jnp.einsum("bhd,bhde->bhe", query_rows, cell_state, precision=highest)
    numerator = weight_old[..., None] * cell_read + weight_new[..., None] * value_rows
    denominator = weight_old * jnp.sum(query_rows * norm_state, axis=-1) + weight_new
    cell_out = numerator / jnp.maximum(jnp.abs(denominator), 1.0)[..., None]
    mixed = (jax.nn.sigmoid(out_gate) * cell_out.reshape(seq_count, -1)).astype(jnp.bfloat16)
    all_heads = collect(mixed, "tp", 1)
    resid = (
        tokens.astype(jnp.float32)
        + jnp.dot(all_heads, w_mix_out, preferred_element_type=jnp.float32)
    ).astype(jnp.bfloat16)
    whole_resid = collect(resid, "tp", 1)
    normed_full = rms_norm(whole_resid, gain_ffn)
    normed_part = lax.dynamic_slice_in_dim(normed_full, tp_rank * quarter, quarter, 1)
    experts = lax.axis_size("ep")
    slots = (2 * seq_count * TOP + experts - 1) // experts
    flat_ids = route_ids.reshape(-1)
    onehot = (flat_ids[:, None] == jnp.arange(experts, dtype=jnp.int32)[None, :]).astype(jnp.int32)
    earlier = jnp.cumsum(onehot, axis=0) - onehot
    slot_rank = jnp.sum(earlier * onehot, axis=1)
    target = flat_ids * slots + slot_rank
    select = (jnp.arange(experts * slots, dtype=jnp.int32)[:, None] == target[None, :]).astype(
        jnp.bfloat16
    )
    repeated = jnp.repeat(normed_full, TOP, axis=0)
    outgoing = jnp.dot(select, repeated, preferred_element_type=jnp.float32).astype(jnp.bfloat16)
    outgoing = outgoing.reshape(experts, slots, -1)
    received = lax.all_to_all(outgoing, "ep", split_axis=0, concat_axis=0, tiled=True)
    sources = received.shape[0]
    item_count = received.shape[1]
    flat_rows = received.reshape(sources * item_count, -1)
    gate_rows = jnp.dot(flat_rows, expert_gate[0], preferred_element_type=jnp.float32)
    up_rows = jnp.dot(flat_rows, expert_up[0], preferred_element_type=jnp.float32)
    hidden = (jax.nn.silu(gate_rows) * up_rows).astype(jnp.bfloat16)
    partial_value = jnp.dot(hidden, expert_down[0], preferred_element_type=jnp.float32)
    summed = sent_and_summed(partial_value.astype(jnp.bfloat16), "tp", 1).astype(jnp.bfloat16)
    returned = lax.all_to_all(
        summed.reshape(sources, item_count, -1), "ep", split_axis=0, concat_axis=0, tiled=True
    )
    picked = lax.dot_general(
        select,
        returned.reshape(experts * slots, -1),
        (((0,), (0,)), ((), ())),
        preferred_element_type=jnp.float32,
    ).reshape(seq_count, TOP, -1)
    route_weight = jax.nn.sigmoid(route_logits - route_logits[:, ::-1])
    moe = jnp.sum(route_weight[..., None] * picked, axis=1)
    mix_part = jnp.dot(normed_part, dense_mix, preferred_element_type=jnp.float32)
    pieces = turned_gather((dense_gate, dense_up), "ep", (1, 1))
    gate_cols = jnp.dot(normed_part, pieces[0], preferred_element_type=jnp.float32)
    up_cols = jnp.dot(normed_part, pieces[1], preferred_element_type=jnp.float32)
    gate_sum, up_sum, mix_logit = (
        of_everyone(gate_cols.astype(jnp.bfloat16), "tp").astype(jnp.float32),
        of_everyone(up_cols.astype(jnp.bfloat16), "tp").astype(jnp.float32),
        of_everyone(mix_part.astype(jnp.bfloat16), "tp").astype(jnp.float32),
    )
    dense_hidden = (jax.nn.silu(gate_sum) * up_sum).astype(jnp.bfloat16)
    dense_out = jnp.dot(
        dense_hidden,
        lax.all_gather(dense_down, "ep", axis=0, tiled=True),
        preferred_element_type=jnp.float32,
    )
    mix_gate = jax.nn.sigmoid(mix_logit)
    total = resid.astype(jnp.float32) + moe + mix_gate[:, None] * dense_out
    return total.astype(jnp.bfloat16)


def solution(mesh):
    return jax.shard_map(
        local,
        mesh=mesh,
        in_specs=(
            P("ep", "tp"),
            P(),
            P(None, "tp"),
            P(None, "tp"),
            P(None, "tp"),
            P(None, "tp"),
            P(None, "tp"),
            P(None, "tp"),
            P(None, "tp"),
            P("ep", "tp", None, None),
            P("ep", "tp", None),
            P("ep", "tp"),
            P(),
            P("ep", None),
            P("ep", None),
            P("ep", None, "tp"),
            P("ep", None, "tp"),
            P("ep", "tp", None),
            P("tp", "ep"),
            P("tp", "ep"),
            P("ep", "tp"),
            P("tp"),
        ),
        out_specs=P("ep", "tp"),
        check_vma=False,
    )
```

profile of v0, /device:TPU:1, one launch (start us, length us, event | category | flops | bytes accessed | tf_op | source)
XLA Modules:
  0.0 192.4 jit_solution(7491865044756722748)
XLA Ops:
  6.5 0.0 all-gather.3.cloned.1.call-start
  6.6 1.4 pad_maximum_fusion
  8.0 1.3 broadcast_in_dim.14
  9.3 4.8 %all-to-all-start = ((bf16[4,16,256]{2,1,0:T(8,128)(2,1)}), bf16[4,16,256]{2,1,0:T(8,128)(2,1)S(1)}, u32[]{:S(2)}, u32[]{:S(2)}) async-start(bf16[4,16,256]{2,1,0:T(8,128)(2,1)} %broadcast_in_dim.14), calls=%async_computation | async-start | bytes 65536 | tf_op jit(solution)/shard_map/all_to_all | solution.py:14
  14.2 0.7 all-gather.5.cloned.1.call-update
  14.9 0.7 mul.148
  15.6 0.8 copy.72
  16.4 0.1 reshape.174
  16.5 2.0 %all-to-all-done = bf16[4,16,256]{2,1,0:T(8,128)(2,1)S(1)} async-done(((bf16[4,16,256]{2,1,0:T(8,128)(2,1)}), bf16[4,16,256]{2,1,0:T(8,128)(2,1)S(1)}, u32[]{:S(2)}, u32[]{:S(2)}) %all-to-all-start) | async-done | bytes 32800 | tf_op jit(solution)/shard_map/all_to_all | solution.py:14
  18.5 0.1 fusion.40
  18.6 0.8 multiply_convert_fusion.3
  19.4 0.1 fusion.45
  19.5 1.1 fusion.14
  20.6 1.2 fusion.51
  21.8 1.2 fusion.16
  23.1 1.0 fusion.19
  24.0 0.1 bitcast_add_fusion
  24.2 0.1 maximum_bitcast_fusion
  24.3 0.2 fusion.15
  24.5 0.6 broadcast_in_dim.15
  25.1 3.2 %all-to-all-start.1 = ((bf16[4,16,128]{2,1,0:T(8,128)(2,1)}), bf16[4,16,128]{2,1,0:T(8,128)(2,1)S(1)}, u32[]{:S(2)}, u32[]{:S(2)}) async-start(bf16[4,16,128]{2,1,0:T(8,128)(2,1)} %broadcast_in_dim.15), calls=%async_computation.1 | async-start | bytes 32768 | tf_op jit(solution)/shard_map/all_to_all | solution.py:14
  28.4 0.1 fusion.49
  28.4 0.1 reduce_window_sum.11
  28.5 4.0 %all-to-all-done.1 = bf16[4,16,128]{2,1,0:T(8,128)(2,1)S(1)} async-done(((bf16[4,16,128]{2,1,0:T(8,128)(2,1)}), bf16[4,16,128]{2,1,0:T(8,128)(2,1)S(1)}, u32[]{:S(2)}, u32[]{:S(2)}) %all-to-all-start.1) | async-done | bytes 16416 | tf_op jit(solution)/shard_map/all_to_all | solution.py:14
  32.5 0.1 fusion.6
  32.7 0.6 broadcast_in_dim.16
  33.3 3.3 %all-to-all-start.2 = ((bf16[4,16,256]{2,1,0:T(8,128)(2,1)}), bf16[4,16,256]{2,1,0:T(8,128)(2,1)S(1)}, u32[]{:S(2)}, u32[]{:S(2)}) async-start(bf16[4,16,256]{2,1,0:T(8,128)(2,1)} %broadcast_in_dim.16), calls=%async_computation.2 | async-start | bytes 65536 | tf_op jit(solution)/shard_map/all_to_all | solution.py:14
  36.6 0.2 select_reduce_fusion
  36.8 4.1 %all-to-all-done.2 = bf16[4,16,256]{2,1,0:T(8,128)(2,1)S(1)} async-done(((bf16[4,16,256]{2,1,0:T(8,128)(2,1)}), bf16[4,16,256]{2,1,0:T(8,128)(2,1)S(1)}, u32[]{:S(2)}, u32[]{:S(2)}) %all-to-all-start.2) | async-done | bytes 32800 | tf_op jit(solution)/shard_map/all_to_all | solution.py:14
  40.8 0.1 fusion.39
  41.0 0.1 multiply_convert_fusion.2
  41.2 0.2 fusion.2
  41.4 0.5 broadcast.120
  41.9 0.7 reduce.9
  42.6 0.9 reshape.195
  43.5 21.3 %all-to-all-start.3 = ((bf16[128,2,512]{2,1,0:T(2,128)(2,1)}), bf16[128,2,512]{2,1,0:T(2,128)(2,1)S(1)}, u32[]{:S(2)}, u32[]{:S(2)}) async-start(bf16[128,2,512]{2,1,0:T(2,128)(2,1)} %reshape.195), calls=%async_computation.3 | async-start | bytes 524288 | tf_op jit(solution)/shard_map/all_to_all | solution.py:133
  64.8 0.1 iota_compare_fusion.3
  65.0 15.1 %all-to-all-done.3 = bf16[128,2,512]{2,1,0:T(2,128)(2,1)S(1)} async-done(((bf16[128,2,512]{2,1,0:T(2,128)(2,1)}), bf16[128,2,512]{2,1,0:T(2,128)(2,1)S(1)}, u32[]{:S(2)}, u32[]{:S(2)}) %all-to-all-start.3) | async-done | bytes 262176 | tf_op jit(solution)/shard_map/all_to_all | solution.py:133
  80.0 0.2 reshape.196
  80.3 0.4 fusion.24
  80.7 2.0 %convolution_convert_fusion.3 = bf16[128,1024]{1,0:T(8,128)(2,1)S(1)} fusion(bf16[1,352,1024]{2,1,0:T(8,128)(2,1)S(1)} %copy-done.6, bf16[1,1024,352]{1,2,0:T(8,128)(2,1)} %param.38, f32[128,352]{0,1:T(8,128)S(1)} %fusion.24, bf16[128,1,1024]{2,1,0:T(2,128)(2,1)S(1)} %reshape.196), kind=kOutput, calls=%fused_computation.5 | convolution fusion | flops 184950784 | bytes 2146304 | tf_op jit(solution)/shard_map/dot_general | solution.py:140
  82.7 0.7 copy.109
  83.4 3.4 %all-to-all-start.4 = ((bf16[4,128,256]{2,1,0:T(8,128)(2,1)}), bf16[4,128,256]{2,1,0:T(8,128)(2,1)S(1)}, u32[]{:S(2)}, u32[]{:S(2)}) async-start(bf16[4,128,256]{2,1,0:T(8,128)(2,1)} %bitcast.113), calls=%async_computation.4 | async-start | bytes 524288 | tf_op jit(solution)/shard_map/all_to_all | solution.py:38
  86.8 0.1 fusion.17
  87.0 6.0 %all-to-all-done.4 = bf16[4,128,256]{2,1,0:T(8,128)(2,1)S(1)} async-done(((bf16[4,128,256]{2,1,0:T(8,128)(2,1)}), bf16[4,128,256]{2,1,0:T(8,128)(2,1)S(1)}, u32[]{:S(2)}, u32[]{:S(2)}) %all-to-all-start.4) | async-done | bytes 262176 | tf_op jit(solution)/shard_map/all_to_all | solution.py:38
  92.9 0.6 broadcast_in_dim.18
  93.5 3.2 %all-to-all-start.6 = ((bf16[4,1,16]{2,1,0:T(2,128)(2,1)}), bf16[4,1,16]{2,1,0:T(2,128)(2,1)S(1)}, u32[]{:S(2)}, u32[]{:S(2)}) async-start(bf16[4,1,16]{2,1,0:T(2,128)(2,1)} %broadcast_in_dim.18), calls=%async_computation.6 | async-start | bytes 4096 | tf_op jit(solution)/shard_map/all_to_all | solution.py:14
  96.8 0.6 reduce.10
  97.4 0.6 reshape.197
  98.0 2.8 %all-to-all-done.6 = bf16[4,1,16]{2,1,0:T(2,128)(2,1)S(1)} async-done(((bf16[4,1,16]{2,1,0:T(2,128)(2,1)}), bf16[4,1,16]{2,1,0:T(2,128)(2,1)S(1)}, u32[]{:S(2)}, u32[]{:S(2)}) %all-to-all-start.6) | async-done | bytes 160 | tf_op jit(solution)/shard_map/all_to_all | solution.py:14
  100.7 7.7 %all-to-all-start.5 = ((bf16[128,2,128]{2,1,0:T(2,128)(2,1)}), bf16[128,2,128]{2,1,0:T(2,128)(2,1)S(1)}, u32[]{:S(2)}, u32[]{:S(2)}) async-start(bf16[128,2,128]{2,1,0:T(2,128)(2,1)} %reshape.197), calls=%async_computation.5 | async-start | bytes 131072 | tf_op jit(solution)/shard_map/all_to_all | solution.py:142
  108.5 1.9 convolution_convert_fusion.1
  110.4 9.6 %all-to-all-done.5 = bf16[128,2,128]{2,1,0:T(2,128)(2,1)S(1)} async-done(((bf16[128,2,128]{2,1,0:T(2,128)(2,1)}), bf16[128,2,128]{2,1,0:T(2,128)(2,1)S(1)}, u32[]{:S(2)}, u32[]{:S(2)}) %all-to-all-start.5) | async-done | bytes 65568 | tf_op jit(solution)/shard_map/all_to_all | solution.py:142
  120.0 0.8 broadcast_in_dim.19
  120.8 3.5 %all-to-all-start.7 = ((bf16[4,16,3072]{2,1,0:T(8,128)(2,1)}), bf16[4,16,3072]{2,1,0:T(8,128)(2,1)S(1)}, u32[]{:S(2)}, u32[]{:S(2)}) async-start(bf16[4,16,3072]{2,1,0:T(8,128)(2,1)} %broadcast_in_dim.19), calls=%async_computation.7 | async-start | bytes 786432 | tf_op jit(solution)/shard_map/all_to_all | solution.py:14
  124.3 1.9 convolution_convert_fusion
  126.2 5.6 %all-to-all-done.7 = bf16[4,16,3072]{2,1,0:T(8,128)(2,1)S(1)} async-done(((bf16[4,16,3072]{2,1,0:T(8,128)(2,1)}), bf16[4,16,3072]{2,1,0:T(8,128)(2,1)S(1)}, u32[]{:S(2)}, u32[]{:S(2)}) %all-to-all-start.7) | async-done | bytes 393248 | tf_op jit(solution)/shard_map/all_to_all | solution.py:14
  131.9 0.8 broadcast_in_dim.20
  132.6 3.5 %all-to-all-start.8 = ((bf16[4,16,3072]{2,1,0:T(8,128)(2,1)}), bf16[4,16,3072]{2,1,0:T(8,128)(2,1)S(1)}, u32[]{:S(2)}, u32[]{:S(2)}) async-start(bf16[4,16,3072]{2,1,0:T(8,128)(2,1)} %broadcast_in_dim.20), calls=%async_computation.8 | async-start | bytes 786432 | tf_op jit(solution)/shard_map/all_to_all | solution.py:14
  136.1 0.1 fusion.4
  136.2 0.1 convert_reduce_fusion.1
  136.3 6.2 %all-to-all-done.8 = bf16[4,16,3072]{2,1,0:T(8,128)(2,1)S(1)} async-done(((bf16[4,16,3072]{2,1,0:T(8,128)(2,1)}), bf16[4,16,3072]{2,1,0:T(8,128)(2,1)S(1)}, u32[]{:S(2)}, u32[]{:S(2)}) %all-to-all-start.8) | async-done | bytes 393248 | tf_op jit(solution)/shard_map/all_to_all | solution.py:14
  142.6 40.6 %all-gather.5.cloned.1.call-done = bf16[3072,256]{1,0:T(8,128)(2,1)} async-done(((bf16[24,256]{1,0:T(8,128)(2,1)}), bf16[3072,256]{1,0:T(8,128)(2,1)}) %all-gather.5.cloned.1.call-update) | async-done | bytes 1572880 | tf_op jit(solution)/shard_map/all_gather | solution.py:165
  183.3 2.3 %fusion.7 = bf16[16,256]{1,0:T(8,128)(2,1)} fusion(bf16[3072,256]{1,0:T(8,128)(2,1)} %all-gather.5.cloned.1.call-done, f32[16,3072]{1,0:T(8,128)S(1)} %convert_reduce_fusion, f32[16,3072]{1,0:T(8,128)S(1)} %convert_reduce_fusion.1, f32[16,256]{1,0:T(8,128)S(1)} %fusion.4, bf16[16,256]{1,0:T(8,128)(2,1)S(1)} %fusion.6, f32[16]{0:T(128)S(1)} %add_divide_fusion.1), kind=kOutput, calls=%fused_computation.15 | convolution fusion | flops 25481216 | bytes 1998912 | tf_op jit(solution)/shard_map/dot_general | solution.py:163
  (46 shorter events, 0.4 us)
Async XLA Ops:
  6.5 16.5 %copy-start = (f32[16,1,128,128]{3,2,1,0:T(8,128)S(1)}, f32[16,1,128,128]{3,2,1,0:T(8,128)}, u32[]{:S(2)}) copy-start(f32[16,1,128,128]{3,2,1,0:T(8,128)} %param.31) | copy-start | bytes 3145732
  6.5 17.5 %copy-start.8 = (bf16[1024,1]{0,1:T(2,128)(2,1)S(1)}, bf16[1024,1]{0,1:T(2,128)(2,1)}, u32[]{:S(2)}) copy-start(bf16[1024,1]{0,1:T(2,128)(2,1)} %param.29) | copy-start | bytes 6148
  6.5 17.5 %copy-start.10 = (f32[16,1]{0,1:T(1,128)S(1)}, f32[16,1]{0,1:T(1,128)}, u32[]{:S(2)}) copy-start(f32[16,1]{0,1:T(1,128)} %param.33) | copy-start | bytes 196
  6.5 17.6 %copy-start.9 = (bf16[1024,1]{0,1:T(2,128)(2,1)S(1)}, bf16[1024,1]{0,1:T(2,128)(2,1)}, u32[]{:S(2)}) copy-start(bf16[1024,1]{0,1:T(2,128)(2,1)} %param.28) | copy-start | bytes 6148
  6.5 17.8 %copy-start.7 = (bf16[1024,128]{1,0:T(8,128)(2,1)S(1)}, bf16[1024,128]{1,0:T(8,128)(2,1)}, u32[]{:S(2)}) copy-start(bf16[1024,128]{1,0:T(8,128)(2,1)} %param.26) | copy-start | bytes 786436
  6.5 101.9 %all-gather.3.cloned.1.call-start = ((), (), s32[]{:S(2)}) async-start(), calls=%async_computation.9 | async-start | bytes 3170304 | tf_op jit(solution)/shard_map/all_gather | solution.py:46
  9.3 9.1 %all-to-all-start = ((bf16[4,16,256]{2,1,0:T(8,128)(2,1)}), bf16[4,16,256]{2,1,0:T(8,128)(2,1)S(1)}, u32[]{:S(2)}, u32[]{:S(2)}) async-start(bf16[4,16,256]{2,1,0:T(8,128)(2,1)} %broadcast_in_dim.14), calls=%async_computation | async-start | bytes 65536 | tf_op jit(solution)/shard_map/all_to_all | solution.py:14
  14.2 18.4 %copy-start.2 = (bf16[512,256]{1,0:T(8,128)(2,1)S(1)}, bf16[512,256]{1,0:T(8,128)(2,1)}, u32[]{:S(2)}) copy-start(bf16[512,256]{1,0:T(8,128)(2,1)} %param.30) | copy-start | bytes 786436
  14.2 18.4 %copy-start.3 = (bf16[16,256]{1,0:T(8,128)(2,1)S(1)}, bf16[16,256]{1,0:T(8,128)(2,1)}, u32[]{:S(2)}) copy-start(bf16[16,256]{1,0:T(8,128)(2,1)} %param.22) | copy-start | bytes 24580
  14.2 169.1 %all-gather.5.cloned.1.call-start = ((), (), s32[]{:S(2)}) async-start(), calls=%async_computation.10 | async-start | bytes 1585152 | tf_op jit(solution)/shard_map/all_gather | solution.py:165
  19.5 21.5 %copy-start.4 = (f32[1024]{0:T(1024)S(1)}, f32[1024]{0:T(1024)}, u32[]{:S(2)}) copy-start(f32[1024]{0:T(1024)} %param.34) | copy-start | bytes 12292
  24.5 40.4 %copy-start.5 = (f32[16,2]{0,1:T(2,128)S(1)}, f32[16,2]{0,1:T(2,128)}, u32[]{:S(2)}) copy-start(f32[16,2]{0,1:T(2,128)} %param.36) | copy-start | bytes 388
  24.5 40.4 %copy-start.11 = (bf16[256]{0:T(256)(128)(2,1)S(1)}, bf16[256]{0:T(256)(128)(2,1)}, u32[]{:S(2)}) copy-start(bf16[256]{0:T(256)(128)(2,1)} %param.43) | copy-start | bytes 1540
  25.1 7.4 %all-to-all-start.1 = ((bf16[4,16,128]{2,1,0:T(8,128)(2,1)}), bf16[4,16,128]{2,1,0:T(8,128)(2,1)S(1)}, u32[]{:S(2)}, u32[]{:S(2)}) async-start(bf16[4,16,128]{2,1,0:T(8,128)(2,1)} %broadcast_in_dim.15), calls=%async_computation.1 | async-start | bytes 32768 | tf_op jit(solution)/shard_map/all_to_all | solution.py:14
  33.3 7.5 %all-to-all-start.2 = ((bf16[4,16,256]{2,1,0:T(8,128)(2,1)}), bf16[4,16,256]{2,1,0:T(8,128)(2,1)S(1)}, u32[]{:S(2)}, u32[]{:S(2)}) async-start(bf16[4,16,256]{2,1,0:T(8,128)(2,1)} %broadcast_in_dim.16), calls=%async_computation.2 | async-start | bytes 65536 | tf_op jit(solution)/shard_map/all_to_all | solution.py:14
  41.0 39.3 %copy-start.1 = (bf16[1,1024,352]{1,2,0:T(8,128)(2,1)S(1)}, bf16[1,1024,352]{1,2,0:T(8,128)(2,1)}, u32[]{:S(2)}) copy-start(bf16[1,1024,352]{1,2,0:T(8,128)(2,1)} %param.37) | copy-start | bytes 2162692
  42.6 38.1 %copy-start.6 = (bf16[1,352,1024]{2,1,0:T(8,128)(2,1)S(1)}, bf16[1,352,1024]{2,1,0:T(8,128)(2,1)}, u32[]{:S(2)}) copy-start(bf16[1,352,1024]{2,1,0:T(8,128)(2,1)} %param.39) | copy-start | bytes 2162692
  43.5 36.6 %all-to-all-start.3 = ((bf16[128,2,512]{2,1,0:T(2,128)(2,1)}), bf16[128,2,512]{2,1,0:T(2,128)(2,1)S(1)}, u32[]{:S(2)}, u32[]{:S(2)}) async-start(bf16[128,2,512]{2,1,0:T(2,128)(2,1)} %reshape.195), calls=%async_computation.3 | async-start | bytes 524288 | tf_op jit(solution)/shard_map/all_to_all | solution.py:133
  83.4 9.5 %all-to-all-start.4 = ((bf16[4,128,256]{2,1,0:T(8,128)(2,1)}), bf16[4,128,256]{2,1,0:T(8,128)(2,1)S(1)}, u32[]{:S(2)}, u32[]{:S(2)}) async-start(bf16[4,128,256]{2,1,0:T(8,128)(2,1)} %bitcast.113), calls=%async_computation.4 | async-start | bytes 524288 | tf_op jit(solution)/shard_map/all_to_all | solution.py:38
  93.5 7.3 %all-to-all-start.6 = ((bf16[4,1,16]{2,1,0:T(2,128)(2,1)}), bf16[4,1,16]{2,1,0:T(2,128)(2,1)S(1)}, u32[]{:S(2)}, u32[]{:S(2)}) async-start(bf16[4,1,16]{2,1,0:T(2,128)(2,1)} %broadcast_in_dim.18), calls=%async_computation.6 | async-start | bytes 4096 | tf_op jit(solution)/shard_map/all_to_all | solution.py:14
  100.7 19.3 %all-to-all-start.5 = ((bf16[128,2,128]{2,1,0:T(2,128)(2,1)}), bf16[128,2,128]{2,1,0:T(2,128)(2,1)S(1)}, u32[]{:S(2)}, u32[]{:S(2)}) async-start(bf16[128,2,128]{2,1,0:T(2,128)(2,1)} %reshape.197), calls=%async_computation.5 | async-start | bytes 131072 | tf_op jit(solution)/shard_map/all_to_all | solution.py:142
  120.8 11.0 %all-to-all-start.7 = ((bf16[4,16,3072]{2,1,0:T(8,128)(2,1)}), bf16[4,16,3072]{2,1,0:T(8,128)(2,1)S(1)}, u32[]{:S(2)}, u32[]{:S(2)}) async-start(bf16[4,16,3072]{2,1,0:T(8,128)(2,1)} %broadcast_in_dim.19), calls=%async_computation.7 | async-start | bytes 786432 | tf_op jit(solution)/shard_map/all_to_all | solution.py:14
  132.6 9.9 %all-to-all-start.8 = ((bf16[4,16,3072]{2,1,0:T(8,128)(2,1)}), bf16[4,16,3072]{2,1,0:T(8,128)(2,1)S(1)}, u32[]{:S(2)}, u32[]{:S(2)}) async-start(bf16[4,16,3072]{2,1,0:T(8,128)(2,1)} %broadcast_in_dim.20), calls=%async_computation.8 | async-start | bytes 786432 | tf_op jit(solution)/shard_map/all_to_all | solution.py:14
Sparse Core Ops, SparseCore 0:
  10.5 90.2 all-gather.2
  104.0 79.2 all-gather.4
where the time goes:
time: 193 us; the launch traced here: 192 us
  waiting for transfers between devices  96.8 us (50%)
  starting transfers between devices  54 us (28%)
  matrix products  14.1 us (7%)
  between operations  13.7 us (7%)
  local copies, waits for them, and re-layouts  9.37 us (5%)
  other arithmetic  4.49 us (2%)
    all_gather x1, waiting for transfers between devices, local(): lax.all_gather(dense_down, 'ep', axis=0, tiled=True)  40.6 us
    all_to_all x6, waiting for transfers between devices, sent_to_all(): lax.all_to_all(jnp.broadcast_to(shard[None], (size, *shard.shape)), axis,...  24.7 us
    all_to_all x6, starting transfers between devices, sent_to_all(): lax.all_to_all(jnp.broadcast_to(shard[None], (size, *shard.shape)), axis,...  21.5 us
    all_to_all x1, starting transfers between devices, local(): lax.all_to_all(outgoing, 'ep', split_axis=0, concat_axis=0, tiled=True)  21.3 us
    all_to_all x1, waiting for transfers between devices, local(): lax.all_to_all(outgoing, 'ep', split_axis=0, concat_axis=0, tiled=True)  15.1 us
    all_to_all x1, waiting for transfers between devices, local(): lax.all_to_all(summed.reshape(sources, item_count, -1), 'ep', split_axis=...  9.63 us
    all_to_all x1, starting transfers between devices, local(): lax.all_to_all(summed.reshape(sources, item_count, -1), 'ep', split_axis=...  7.71 us
    all_to_all x1, waiting for transfers between devices, sent_and_summed(): lax.all_to_all(blocks, axis, split_axis=0, concat_axis=0, tiled=True)  5.95 us
  transfers between devices with their start and end apart: 11, of which 10 were waited for; matrix products, arithmetic and copies ran while one was open for 13% of the time, Pallas kernels for 0%

commit v1 on v0

--- a/solution.py
+++ b/solution.py
@@ -1,12 +1,24 @@
+import functools
 import jax
 import jax.numpy as jnp
 from jax import lax
 from jax.sharding import PartitionSpec as P
+from jax.lax import all_to_all, axis_size
 
 HEAD = 128
 TOP = 2
 epsilon = 1e-06
 highest = lax.Precision.HIGHEST
+
+
+def divide_the_lane(piece_in, shard_axis):
+    z2 = jnp.concatenate(
+        all_to_all(jnp.stack([piece_in] * axis_size(shard_axis)), shard_axis, 0, 0), 0
+    )
+    return z2
+
+
+put_the_rings = functools.partial(divide_the_lane, shard_axis="ep")
 
 
 def sent_to_all(shard, axis):
@@ -160,11 +172,7 @@
         of_everyone(mix_part.astype(jnp.bfloat16), "tp").astype(jnp.float32),
     )
     dense_hidden = (jax.nn.silu(gate_sum) * up_sum).astype(jnp.bfloat16)
-    dense_out = jnp.dot(
-        dense_hidden,
-        lax.all_gather(dense_down, "ep", axis=0, tiled=True),
-        preferred_element_type=jnp.float32,
-    )
+    dense_out = jnp.dot(dense_hidden, put_the_rings(dense_down), preferred_element_type=jnp.float32)
     mix_gate = jax.nn.sigmoid(mix_logit)
     total = resid.astype(jnp.float32) + moe + mix_gate[:, None] * dense_out
     return total.astype(jnp.bfloat16)

time: 193 us -> 203 us (1.052)
  blocking collectives: 0 us -> 8.62 us
  waiting for transfers between devices: 96.8 us -> 89.5 us
  starting transfers between devices: 54 us -> 58.1 us
    all_gather x1 -> x0, waiting for transfers between devices: 40.6 us -> none  [local(): lax.all_gather(dense_down, 'ep', axis=0, tiled=True)]
    all_to_all x0 -> x1, waiting for transfers between devices: none -> 38.7 us  [divide_the_lane(): all_to_all(jnp.stack([piece_in] * axis_size(shard_axis)), shard_axis, 0, 0)]
    all_to_all x0 -> x1, blocking collectives: none -> 8.62 us  [sent_to_all(): lax.all_to_all(jnp.broadcast_to(shard[None], (size, *shard.shape)), axis,...]
    all_to_all x0 -> x1, starting transfers between devices: none -> 8.22 us  [divide_the_lane(): all_to_all(jnp.stack([piece_in] * axis_size(shard_axis)), shard_axis, 0, 0)]
    all_to_all x6 -> x5, waiting for transfers between devices: 24.7 us -> 18.8 us  [sent_to_all(): lax.all_to_all(jnp.broadcast_to(shard[None], (size, *shard.shape)), axis,...]
    all_to_all x6 -> x5, starting transfers between devices: 21.5 us -> 18 us  [sent_to_all(): lax.all_to_all(jnp.broadcast_to(shard[None], (size, *shard.shape)), axis,...]
  transfers between devices with their start and end apart: 11 -> 10, of which waited for: 10 -> 9; matrix products, arithmetic and copies ran while one was open for 13% -> 13% of each run, Pallas kernels for 0% -> 0%
where the time goes in v1:
time: 203 us; the launch traced here: 202 us
  waiting for transfers between devices  89.5 us (44%)
  starting transfers between devices  58.1 us (29%)
  matrix products  15.9 us (8%)
  between operations  13.7 us (7%)
  local copies, waits for them, and re-layouts  10.7 us (5%)
  blocking collectives  8.62 us (4%)
  other arithmetic  5.44 us (3%)
    all_to_all x1, waiting for transfers between devices, divide_the_lane(): all_to_all(jnp.stack([piece_in] * axis_size(shard_axis)), shard_axis, 0, 0)  38.7 us
    all_to_all x1, starting transfers between devices, local(): lax.all_to_all(outgoing, 'ep', split_axis=0, concat_axis=0, tiled=True)  21.3 us
    all_to_all x5, waiting for transfers between devices, sent_to_all(): lax.all_to_all(jnp.broadcast_to(shard[None], (size, *shard.shape)), axis,...  18.8 us
    all_to_all x5, starting transfers between devices, sent_to_all(): lax.all_to_all(jnp.broadcast_to(shard[None], (size, *shard.shape)), axis,...  18 us
    all_to_all x1, waiting for transfers between devices, local(): lax.all_to_all(outgoing, 'ep', split_axis=0, concat_axis=0, tiled=True)  15.9 us
    all_to_all x1, waiting for transfers between devices, local(): lax.all_to_all(summed.reshape(sources, item_count, -1), 'ep', split_axis=...  9.63 us
    all_to_all x1, blocking collectives, sent_to_all(): lax.all_to_all(jnp.broadcast_to(shard[None], (size, *shard.shape)), axis,...  8.62 us
    all_to_all x1, starting transfers between devices, divide_the_lane(): all_to_all(jnp.stack([piece_in] * axis_size(shard_axis)), shard_axis, 0, 0)  8.22 us
  transfers between devices with their start and end apart: 10, of which 9 were waited for; matrix products, arithmetic and copies ran while one was open for 13% of the time, Pallas kernels for 0%

profile of v1, /device:TPU:1, one launch (start us, length us, event | category | flops | bytes accessed | tf_op | source)
XLA Modules:
  0.0 201.9 jit_solution(18098796925456230521)
XLA Ops:
  6.5 1.4 pad_maximum_fusion
  8.0 1.3 broadcast_in_dim.14
  9.3 4.8 %all-to-all-start = ((bf16[4,16,256]{2,1,0:T(8,128)(2,1)}), bf16[4,16,256]{2,1,0:T(8,128)(2,1)S(1)}, u32[]{:S(2)}, u32[]{:S(2)}) async-start(bf16[4,16,256]{2,1,0:T(8,128)(2,1)} %broadcast_in_dim.14), calls=%async_computation | async-start | bytes 65536 | tf_op jit(solution)/shard_map/all_to_all | solution.py:26
  14.1 0.7 mul.148
  14.9 0.8 copy.72
  15.6 0.1 reshape.179
  15.7 2.7 %all-to-all-done = bf16[4,16,256]{2,1,0:T(8,128)(2,1)S(1)} async-done(((bf16[4,16,256]{2,1,0:T(8,128)(2,1)}), bf16[4,16,256]{2,1,0:T(8,128)(2,1)S(1)}, u32[]{:S(2)}, u32[]{:S(2)}) %all-to-all-start) | async-done | bytes 32800 | tf_op jit(solution)/shard_map/all_to_all | solution.py:26
  18.4 0.1 fusion.40
  18.6 0.1 fusion.45
  18.7 0.8 multiply_convert_fusion.3
  19.5 1.2 fusion.51
  20.7 1.2 fusion.16
  21.9 0.8 bitcast_add_fusion
  22.7 0.8 maximum_bitcast_fusion
  23.6 1.1 fusion.14
  24.7 1.0 fusion.19
  25.7 0.2 fusion.15
  25.8 0.6 broadcast_in_dim.15
  26.4 3.2 %all-to-all-start.1 = ((bf16[4,16,128]{2,1,0:T(8,128)(2,1)}), bf16[4,16,128]{2,1,0:T(8,128)(2,1)S(1)}, u32[]{:S(2)}, u32[]{:S(2)}) async-start(bf16[4,16,128]{2,1,0:T(8,128)(2,1)} %broadcast_in_dim.15), calls=%async_computation.1 | async-start | bytes 32768 | tf_op jit(solution)/shard_map/all_to_all | solution.py:26
  29.7 0.1 fusion.49
  29.8 0.1 reduce_window_sum.11
  29.8 4.0 %all-to-all-done.1 = bf16[4,16,128]{2,1,0:T(8,128)(2,1)S(1)} async-done(((bf16[4,16,128]{2,1,0:T(8,128)(2,1)}), bf16[4,16,128]{2,1,0:T(8,128)(2,1)S(1)}, u32[]{:S(2)}, u32[]{:S(2)}) %all-to-all-start.1) | async-done | bytes 16416 | tf_op jit(solution)/shard_map/all_to_all | solution.py:26
  33.9 0.2 fusion.6
  34.0 0.6 broadcast_in_dim.16
  34.6 3.3 %all-to-all-start.2 = ((bf16[4,16,256]{2,1,0:T(8,128)(2,1)}), bf16[4,16,256]{2,1,0:T(8,128)(2,1)S(1)}, u32[]{:S(2)}, u32[]{:S(2)}) async-start(bf16[4,16,256]{2,1,0:T(8,128)(2,1)} %broadcast_in_dim.16), calls=%async_computation.2 | async-start | bytes 65536 | tf_op jit(solution)/shard_map/all_to_all | solution.py:26
  37.9 0.2 select_reduce_fusion
  38.1 4.1 %all-to-all-done.2 = bf16[4,16,256]{2,1,0:T(8,128)(2,1)S(1)} async-done(((bf16[4,16,256]{2,1,0:T(8,128)(2,1)}), bf16[4,16,256]{2,1,0:T(8,128)(2,1)S(1)}, u32[]{:S(2)}, u32[]{:S(2)}) %all-to-all-start.2) | async-done | bytes 32800 | tf_op jit(solution)/shard_map/all_to_all | solution.py:26
  42.2 0.1 fusion.39
  42.3 0.1 multiply_convert_fusion.2
  42.5 0.2 fusion.2
  42.7 0.6 broadcast.122
  43.3 0.8 reduce.9
  44.1 0.9 reshape.201
  45.0 21.3 %all-to-all-start.3 = ((bf16[128,2,512]{2,1,0:T(2,128)(2,1)}), bf16[128,2,512]{2,1,0:T(2,128)(2,1)S(1)}, u32[]{:S(2)}, u32[]{:S(2)}) async-start(bf16[128,2,512]{2,1,0:T(2,128)(2,1)} %reshape.201), calls=%async_computation.3 | async-start | bytes 524288 | tf_op jit(solution)/shard_map/all_to_all | solution.py:145
  66.4 15.9 %all-to-all-done.3 = bf16[128,2,512]{2,1,0:T(2,128)(2,1)S(1)} async-done(((bf16[128,2,512]{2,1,0:T(2,128)(2,1)}), bf16[128,2,512]{2,1,0:T(2,128)(2,1)S(1)}, u32[]{:S(2)}, u32[]{:S(2)}) %all-to-all-start.3) | async-done | bytes 262176 | tf_op jit(solution)/shard_map/all_to_all | solution.py:145
  82.3 0.2 reshape.202
  82.5 0.4 fusion.24
  82.9 2.0 convolution_convert_fusion.3
  84.9 0.7 copy.109
  85.7 3.4 %all-to-all-start.4 = ((bf16[4,128,256]{2,1,0:T(8,128)(2,1)}), bf16[4,128,256]{2,1,0:T(8,128)(2,1)S(1)}, u32[]{:S(2)}, u32[]{:S(2)}) async-start(bf16[4,128,256]{2,1,0:T(8,128)(2,1)} %bitcast.114), calls=%async_computation.4 | async-start | bytes 524288 | tf_op jit(solution)/shard_map/all_to_all | solution.py:50
  89.1 0.1 fusion.17
  89.2 6.5 %all-to-all-done.4 = bf16[4,128,256]{2,1,0:T(8,128)(2,1)S(1)} async-done(((bf16[4,128,256]{2,1,0:T(8,128)(2,1)}), bf16[4,128,256]{2,1,0:T(8,128)(2,1)S(1)}, u32[]{:S(2)}, u32[]{:S(2)}) %all-to-all-start.4) | async-done | bytes 262176 | tf_op jit(solution)/shard_map/all_to_all | solution.py:50
  95.7 0.6 broadcast_in_dim.18
  96.3 3.2 %all-to-all-start.6 = ((bf16[4,1,16]{2,1,0:T(2,128)(2,1)}), bf16[4,1,16]{2,1,0:T(2,128)(2,1)S(1)}, u32[]{:S(2)}, u32[]{:S(2)}) async-start(bf16[4,1,16]{2,1,0:T(2,128)(2,1)} %broadcast_in_dim.18), calls=%async_computation.6 | async-start | bytes 4096 | tf_op jit(solution)/shard_map/all_to_all | solution.py:26
  99.5 0.7 reduce.10
  100.3 0.6 reshape.203
  100.9 2.6 %all-to-all-done.6 = bf16[4,1,16]{2,1,0:T(2,128)(2,1)S(1)} async-done(((bf16[4,1,16]{2,1,0:T(2,128)(2,1)}), bf16[4,1,16]{2,1,0:T(2,128)(2,1)S(1)}, u32[]{:S(2)}, u32[]{:S(2)}) %all-to-all-start.6) | async-done | bytes 160 | tf_op jit(solution)/shard_map/all_to_all | solution.py:26
  103.5 7.2 %all-to-all-start.5 = ((bf16[128,2,128]{2,1,0:T(2,128)(2,1)}), bf16[128,2,128]{2,1,0:T(2,128)(2,1)S(1)}, u32[]{:S(2)}, u32[]{:S(2)}) async-start(bf16[128,2,128]{2,1,0:T(2,128)(2,1)} %reshape.203), calls=%async_computation.5 | async-start | bytes 131072 | tf_op jit(solution)/shard_map/all_to_all | solution.py:154
  110.7 0.0 all-gather.2.cloned.1.call-done
  110.7 1.9 convolution_convert_fusion
  112.7 9.6 %all-to-all-done.5 = bf16[128,2,128]{2,1,0:T(2,128)(2,1)S(1)} async-done(((bf16[128,2,128]{2,1,0:T(2,128)(2,1)}), bf16[128,2,128]{2,1,0:T(2,128)(2,1)S(1)}, u32[]{:S(2)}, u32[]{:S(2)}) %all-to-all-start.5) | async-done | bytes 65568 | tf_op jit(solution)/shard_map/all_to_all | solution.py:154
  122.3 0.8 broadcast_in_dim.20
  123.1 3.5 %all-to-all-start.8 = ((bf16[4,16,3072]{2,1,0:T(8,128)(2,1)}), bf16[4,16,3072]{2,1,0:T(8,128)(2,1)S(1)}, u32[]{:S(2)}, u32[]{:S(2)}) async-start(bf16[4,16,3072]{2,1,0:T(8,128)(2,1)} %broadcast_in_dim.20), calls=%async_computation.8 | async-start | bytes 786432 | tf_op jit(solution)/shard_map/all_to_all | solution.py:26
  126.5 1.9 convolution_convert_fusion.1
  128.5 5.3 %all-to-all-done.8 = bf16[4,16,3072]{2,1,0:T(8,128)(2,1)S(1)} async-done(((bf16[4,16,3072]{2,1,0:T(8,128)(2,1)}), bf16[4,16,3072]{2,1,0:T(8,128)(2,1)S(1)}, u32[]{:S(2)}, u32[]{:S(2)}) %all-to-all-start.8) | async-done | bytes 393248 | tf_op jit(solution)/shard_map/all_to_all | solution.py:26
  133.8 8.6 %all_to_all.51 = bf16[4,16,3072]{2,1,0:T(8,128)(2,1)S(1)} all-to-all(bf16[4,16,3072]{2,1,0:T(8,128)(2,1)S(1)} %broadcast_in_dim.19), channel_id=1, replica_groups=mesh['ep'=128,'tp'=4] {'tp'}, dimensions={0} | all-to-all | bytes 786432 | tf_op jit(solution)/shard_map/all_to_all | solution.py:26
  142.4 1.3 stack.2
  143.7 8.2 %all-to-all-start.9 = ((bf16[128,24,256]{2,1,0:T(8,128)(2,1)}), bf16[128,24,256]{2,1,0:T(8,128)(2,1)S(1)}, u32[]{:S(2)}, u32[]{:S(2)}) async-start(bf16[128,24,256]{2,1,0:T(8,128)(2,1)} %stack.2), calls=%async_computation.9 | async-start | bytes 3145728 | tf_op jit(solution)/shard_map/all_to_all | solution.py:16
  152.0 0.1 iota_compare_fusion.3
  152.1 0.7 reshape.204
  152.8 1.0 fusion.4
  153.8 0.8 convert_reduce_fusion
  154.6 38.7 %all-to-all-done.9 = bf16[128,24,256]{2,1,0:T(8,128)(2,1)S(1)} async-done(((bf16[128,24,256]{2,1,0:T(8,128)(2,1)}), bf16[128,24,256]{2,1,0:T(8,128)(2,1)S(1)}, u32[]{:S(2)}, u32[]{:S(2)}) %all-to-all-start.9) | async-done | bytes 1572896 | tf_op jit(solution)/shard_map/all_to_all | solution.py:16
  193.2 1.8 fusion.7
  (41 shorter events, 0.4 us)
Async XLA Ops:
  6.5 18.1 %copy-start = (f32[16,1,128,128]{3,2,1,0:T(8,128)S(1)}, f32[16,1,128,128]{3,2,1,0:T(8,128)}, u32[]{:S(2)}) copy-start(f32[16,1,128,128]{3,2,1,0:T(8,128)} %param.31) | copy-start | bytes 3145732
  6.5 19.1 %copy-start.8 = (bf16[1024,128]{1,0:T(8,128)(2,1)S(1)}, bf16[1024,128]{1,0:T(8,128)(2,1)}, u32[]{:S(2)}) copy-start(bf16[1024,128]{1,0:T(8,128)(2,1)} %param.26) | copy-start | bytes 786436
  6.5 104.2 %all-gather.2.cloned.1.call-start = ((), (), s32[]{:S(2)}) async-start(), calls=%async_computation.10 | async-start | bytes 3170304 | tf_op jit(solution)/shard_map/all_gather | solution.py:58
  9.3 9.1 %all-to-all-start = ((bf16[4,16,256]{2,1,0:T(8,128)(2,1)}), bf16[4,16,256]{2,1,0:T(8,128)(2,1)S(1)}, u32[]{:S(2)}, u32[]{:S(2)}) async-start(bf16[4,16,256]{2,1,0:T(8,128)(2,1)} %broadcast_in_dim.14), calls=%async_computation | async-start | bytes 65536 | tf_op jit(solution)/shard_map/all_to_all | solution.py:26
  14.1 19.7 %copy-start.2 = (bf16[512,256]{1,0:T(8,128)(2,1)S(1)}, bf16[512,256]{1,0:T(8,128)(2,1)}, u32[]{:S(2)}) copy-start(bf16[512,256]{1,0:T(8,128)(2,1)} %param.30) | copy-start | bytes 786436
  14.1 19.7 %copy-start.3 = (bf16[16,256]{1,0:T(8,128)(2,1)S(1)}, bf16[16,256]{1,0:T(8,128)(2,1)}, u32[]{:S(2)}) copy-start(bf16[16,256]{1,0:T(8,128)(2,1)} %param.22) | copy-start | bytes 24580
  19.4 22.9 %copy-start.5 = (f32[1024]{0:T(1024)S(1)}, f32[1024]{0:T(1024)}, u32[]{:S(2)}) copy-start(f32[1024]{0:T(1024)} %param.34) | copy-start | bytes 12292
  25.8 40.6 %copy-start.9 = (bf16[256]{0:T(256)(128)(2,1)S(1)}, bf16[256]{0:T(256)(128)(2,1)}, u32[]{:S(2)}) copy-start(bf16[256]{0:T(256)(128)(2,1)} %param.43) | copy-start | bytes 1540
  26.4 7.4 %all-to-all-start.1 = ((bf16[4,16,128]{2,1,0:T(8,128)(2,1)}), bf16[4,16,128]{2,1,0:T(8,128)(2,1)S(1)}, u32[]{:S(2)}, u32[]{:S(2)}) async-start(bf16[4,16,128]{2,1,0:T(8,128)(2,1)} %broadcast_in_dim.15), calls=%async_computation.1 | async-start | bytes 32768 | tf_op jit(solution)/shard_map/all_to_all | solution.py:26
  34.6 7.5 %all-to-all-start.2 = ((bf16[4,16,256]{2,1,0:T(8,128)(2,1)}), bf16[4,16,256]{2,1,0:T(8,128)(2,1)S(1)}, u32[]{:S(2)}, u32[]{:S(2)}) async-start(bf16[4,16,256]{2,1,0:T(8,128)(2,1)} %broadcast_in_dim.16), calls=%async_computation.2 | async-start | bytes 65536 | tf_op jit(solution)/shard_map/all_to_all | solution.py:26
  42.2 40.3 %copy-start.1 = (bf16[1,1024,352]{1,2,0:T(8,128)(2,1)S(1)}, bf16[1,1024,352]{1,2,0:T(8,128)(2,1)}, u32[]{:S(2)}) copy-start(bf16[1,1024,352]{1,2,0:T(8,128)(2,1)} %param.37) | copy-start | bytes 2162692
  44.1 38.8 %copy-start.7 = (bf16[1,352,1024]{2,1,0:T(8,128)(2,1)S(1)}, bf16[1,352,1024]{2,1,0:T(8,128)(2,1)}, u32[]{:S(2)}) copy-start(bf16[1,352,1024]{2,1,0:T(8,128)(2,1)} %param.39) | copy-start | bytes 2162692
  45.0 37.2 %all-to-all-start.3 = ((bf16[128,2,512]{2,1,0:T(2,128)(2,1)}), bf16[128,2,512]{2,1,0:T(2,128)(2,1)S(1)}, u32[]{:S(2)}, u32[]{:S(2)}) async-start(bf16[128,2,512]{2,1,0:T(2,128)(2,1)} %reshape.201), calls=%async_computation.3 | async-start | bytes 524288 | tf_op jit(solution)/shard_map/all_to_all | solution.py:145
  85.7 10.0 %all-to-all-start.4 = ((bf16[4,128,256]{2,1,0:T(8,128)(2,1)}), bf16[4,128,256]{2,1,0:T(8,128)(2,1)S(1)}, u32[]{:S(2)}, u32[]{:S(2)}) async-start(bf16[4,128,256]{2,1,0:T(8,128)(2,1)} %bitcast.114), calls=%async_computation.4 | async-start | bytes 524288 | tf_op jit(solution)/shard_map/all_to_all | solution.py:50
  96.3 7.3 %all-to-all-start.6 = ((bf16[4,1,16]{2,1,0:T(2,128)(2,1)}), bf16[4,1,16]{2,1,0:T(2,128)(2,1)S(1)}, u32[]{:S(2)}, u32[]{:S(2)}) async-start(bf16[4,1,16]{2,1,0:T(2,128)(2,1)} %broadcast_in_dim.18), calls=%async_computation.6 | async-start | bytes 4096 | tf_op jit(solution)/shard_map/all_to_all | solution.py:26
  103.5 18.8 %all-to-all-start.5 = ((bf16[128,2,128]{2,1,0:T(2,128)(2,1)}), bf16[128,2,128]{2,1,0:T(2,128)(2,1)S(1)}, u32[]{:S(2)}, u32[]{:S(2)}) async-start(bf16[128,2,128]{2,1,0:T(2,128)(2,1)} %reshape.203), calls=%async_computation.5 | async-start | bytes 131072 | tf_op jit(solution)/shard_map/all_to_all | solution.py:154
  123.1 10.7 %all-to-all-start.8 = ((bf16[4,16,3072]{2,1,0:T(8,128)(2,1)}), bf16[4,16,3072]{2,1,0:T(8,128)(2,1)S(1)}, u32[]{:S(2)}, u32[]{:S(2)}) async-start(bf16[4,16,3072]{2,1,0:T(8,128)(2,1)} %broadcast_in_dim.20), calls=%async_computation.8 | async-start | bytes 786432 | tf_op jit(solution)/shard_map/all_to_all | solution.py:26
  126.5 15.9 %copy-start.4 = (bf16[24,256]{1,0:T(8,128)(2,1)S(1)}, bf16[24,256]{1,0:T(8,128)(2,1)}, u32[]{:S(2)}) copy-start(bf16[24,256]{1,0:T(8,128)(2,1)} %param.42) | copy-start | bytes 36868
  143.7 8.2 %copy-start.6 = (f32[16,2]{0,1:T(2,128)S(1)}, f32[16,2]{0,1:T(2,128)}, u32[]{:S(2)}) copy-start(f32[16,2]{0,1:T(2,128)} %param.36) | copy-start | bytes 388
  143.7 49.5 %all-to-all-start.9 = ((bf16[128,24,256]{2,1,0:T(8,128)(2,1)}), bf16[128,24,256]{2,1,0:T(8,128)(2,1)S(1)}, u32[]{:S(2)}, u32[]{:S(2)}) async-start(bf16[128,24,256]{2,1,0:T(8,128)(2,1)} %stack.2), calls=%async_computation.9 | async-start | bytes 3145728 | tf_op jit(solution)/shard_map/all_to_all | solution.py:16
Sparse Core Ops, SparseCore 0:
  10.5 91.1 all-gather.1
